TPU v7x, 32 devices: a whole 2x2x4 slice. The times are simulated.
32 devices in a mesh: sp: 8 (over z, y), tp: 4 (over x, core).
Axes of the slice: x: 2, y: 2, z: 4, core: 2. Of those that a mesh axis runs over, the one named last changes fastest.
Arguments:
- residual: bfloat16 [2048, 2048], P(('sp', 'tp')), may hold values from -6 to 6
- queries: bfloat16 [2048, 2048], P('sp', 'tp'), may hold values from -40 to 40
- key_rows: bfloat16 [2048, 1024], P('sp', 'tp'), may hold values from -40 to 40
- value_rows: bfloat16 [2048, 1024], P('sp', 'tp'), may hold values from -6 to 6
- forget_sums: float32 [2048, 16], P('sp', 'tp'), as said below
- out_weight: bfloat16 [2048, 2048], P('tp'), may hold values from -0.25 to 0.25
- norm_gain: float32 [2048], replicated, may hold values from 0.1 to 1.9
- expert_ids: int32 [2048, 4], P(('sp', 'tp')), may hold values from 0 to 7, all different within a row; in each aligned block of 64 rows (0 to 63, 64 to 127, ...) at most 64 rows name the same one
- route_weights: float32 [2048, 4], P(('sp', 'tp')), may hold values from 0.1 to 1
- expert_gate: bfloat16 [8, 2048, 384], P('sp'), may hold values from -0.125 to 0.125
- expert_up: bfloat16 [8, 2048, 384], P('sp'), may hold values from -0.125 to 0.125
- expert_down: bfloat16 [8, 384, 2048], P('sp'), may hold values from -0.3125 to 0.3125
- shared_gate: bfloat16 [2048, 384], replicated, may hold values from -0.125 to 0.125
- shared_up: bfloat16 [2048, 384], replicated, may hold values from -0.125 to 0.125
- shared_down: bfloat16 [384, 2048], replicated, may hold values from -0.3125 to 0.3125
Outputs:
- layer_out: bfloat16 [2048, 2048], P(('sp', 'tp'))
Inputs may be any that keep to these rules, and one draw needn't show every extreme that they name: `forget_sums`: each head's column never rises from one position to the next. `expert_ids`: each row names 4 different experts; among the rows of one device no expert is named more than 64 times.
All inputs are finite; a program needn't handle non-finite values.
Results may differ from a plain program's by a relative error of at most 0.014.
Values may be sent and summed in bfloat16 or wider, within the bound.
A program may use at most 128 MiB of HBM per device.

v0:
```python
import math
import jax
import jax.numpy as jnp
from jax import lax
from jax.sharding import PartitionSpec as P

HEADS = 16
KV_HEADS = 8
HEAD_DIM = 128
TOPK = 4
routed_scale = 2.5
norm_eps = 1e-06


def absorb_group(carried, query_group, shard_piece, sum_piece, score_scale):
    query_heads, query_sums, query_pos, last_pos = query_group
    key_piece, value_piece = shard_piece
    piece_rows = key_piece.shape[0]
    query_count, local_kv, group_size, head_size = query_heads.shape
    key_block = math.gcd(piece_rows, 1024)
    key_heads = key_piece.reshape(piece_rows, local_kv, head_size)
    value_heads = value_piece.reshape(piece_rows, local_kv, head_size)
    key_sums = sum_piece.reshape(piece_rows, local_kv, group_size).transpose(1, 2, 0)

    def update(block_start, held):
        row_max, row_sum, weighted = held
        key_part = lax.dynamic_slice_in_dim(key_heads, block_start, key_block, 0)
        value_part = lax.dynamic_slice_in_dim(value_heads, block_start, key_block, 0)
        sums_part = lax.dynamic_slice_in_dim(key_sums, block_start, key_block, 2)
        scores = (
            jnp.einsum("qhgd,khd->hgqk", query_heads, key_part, preferred_element_type=jnp.float32)
            * score_scale
        )
        scores = scores + (query_sums[:, :, :, None] - sums_part[:, :, None, :])
        key_pos = block_start + jnp.arange(key_block, dtype=jnp.int32)
        allowed = query_pos[:, None] >= key_pos[None, :]
        scores = jnp.where(allowed, scores, -jnp.inf)
        new_max = jnp.maximum(row_max, jnp.max(scores, axis=3))
        weights = jnp.exp(scores - new_max[:, :, :, None])
        factor = jnp.exp(row_max - new_max)
        row_sum = row_sum * factor + jnp.sum(weights, axis=3)
        products = jnp.einsum(
            "hgqk,khd->qhgd",
            weights.astype(jnp.bfloat16),
            value_part,
            preferred_element_type=jnp.float32,
        )
        weighted = weighted * factor.transpose(2, 0, 1)[:, :, :, None] + products
        return (new_max, row_sum, weighted)

    def one_block(block_index, held):
        block_start = block_index * key_block
        needed = block_start <= last_pos
        return lax.cond(needed, lambda inner: update(block_start, inner), lambda inner: inner, held)

    return lax.fori_loop(0, piece_rows // key_block, one_block, carried)


def finish(carried):
    row_max, row_sum, weighted = carried
    mixed = weighted / row_sum.transpose(2, 0, 1)[:, :, :, None]
    return mixed.reshape(mixed.shape[0], -1).astype(jnp.bfloat16)


def local(
    residual,
    queries,
    key_rows,
    value_rows,
    forget_sums,
    out_weight,
    norm_gain,
    expert_ids,
    route_weights,
    expert_gate,
    expert_up,
    expert_down,
    shared_gate,
    shared_up,
    shared_down,
):
    sp_count = lax.axis_size("sp")
    sp_index = lax.axis_index("sp")
    local_rows = queries.shape[0]
    local_kv = key_rows.shape[1] // HEAD_DIM
    group_size = HEADS // KV_HEADS
    score_scale = HEAD_DIM ** (-0.5)
    own_first = sp_index * local_rows
    all_sums = lax.all_gather(forget_sums, "sp", axis=0, tiled=True)
    positions = own_first + jnp.arange(local_rows, dtype=jnp.int32)
    groups = [
        (
            queries.reshape(queries.shape[0], local_kv, group_size, HEAD_DIM),
            forget_sums.reshape(forget_sums.shape[0], local_kv, group_size).transpose(1, 2, 0),
            positions,
            positions[-1],
        )
    ]

    def initial(query_count):
        return (
            jnp.full((local_kv, group_size, query_count), -1e30, jnp.float32),
            jnp.zeros((local_kv, group_size, query_count), jnp.float32),
            jnp.zeros((query_count, local_kv, group_size, HEAD_DIM), jnp.float32),
        )

    def absorb(states, shard_piece):
        return tuple(
            (
                absorb_group(held, query_group, shard_piece, all_sums, score_scale)
                for held, query_group in zip(states, groups)
            )
        )

    start_states = tuple((initial(query_group[0].shape[0]) for query_group in groups))
    states = absorb(
        start_states,
        (
            lax.all_gather(key_rows, "sp", axis=0, tiled=True),
            lax.all_gather(value_rows, "sp", axis=0, tiled=True),
        ),
    )
    outputs = [finish(held) for held in states]
    attended = outputs[0]
    rows_out = local_rows // lax.axis_size("tp")
    branch = lax.psum_scatter(
        jnp.dot(attended, out_weight, preferred_element_type=jnp.float32).astype(jnp.bfloat16),
        "tp",
        scatter_dimension=0,
        tiled=True,
    ).astype(jnp.float32)
    stream = (residual.astype(jnp.float32) + branch).astype(jnp.bfloat16)
    wide = lax.optimization_barrier(stream).astype(jnp.float32)
    normed = (
        wide * lax.rsqrt(jnp.mean(wide * wide, axis=1, keepdims=True) + norm_eps) * norm_gain
    ).astype(jnp.bfloat16)
    width = normed.shape[1]
    experts_here = expert_gate.shape[0]
    total_experts = experts_here * sp_count
    capacity = 2 * rows_out * TOPK // total_experts
    flat_ids = expert_ids.reshape(-1)
    assigned = flat_ids.shape[0]
    onehot = (flat_ids[:, None] == jnp.arange(total_experts, dtype=jnp.int32)[None, :]).astype(
        jnp.int32
    )
    slot_rank = jnp.sum((jnp.cumsum(onehot, axis=0) - 1) * onehot, axis=1)
    target = flat_ids * capacity + slot_rank
    slot_count = total_experts * capacity
    source = (
        jnp.full((slot_count,), assigned, jnp.int32)
        .at[target]
        .set(jnp.arange(assigned, dtype=jnp.int32))
    )
    padded = jnp.concatenate([normed, jnp.zeros((1, width), jnp.bfloat16)], axis=0)
    outgoing = padded[source // TOPK].reshape(sp_count, experts_here, capacity, width)
    arrived = lax.all_to_all(outgoing, "sp", split_axis=0, concat_axis=0, tiled=True)
    gate_part = jnp.einsum(
        "necd,edf->necf", arrived, expert_gate, preferred_element_type=jnp.float32
    )
    up_part = jnp.einsum("necd,edf->necf", arrived, expert_up, preferred_element_type=jnp.float32)
    hidden = (jax.nn.silu(gate_part) * up_part).astype(jnp.bfloat16)
    processed = jnp.einsum(
        "necf,efd->necd", hidden, expert_down, preferred_element_type=jnp.float32
    ).astype(jnp.bfloat16)
    returned = lax.all_to_all(processed, "sp", split_axis=0, concat_axis=0, tiled=True)
    results = returned.reshape(slot_count, width)
    picked = results[target].reshape(rows_out, TOPK, width).astype(jnp.float32)
    gates = route_weights / jnp.sum(route_weights, axis=1, keepdims=True) * routed_scale
    routed = jnp.sum(gates[:, :, None] * picked, axis=1)
    shared_hidden = (
        jax.nn.silu(jnp.dot(normed, shared_gate, preferred_element_type=jnp.float32))
        * jnp.dot(normed, shared_up, preferred_element_type=jnp.float32)
    ).astype(jnp.bfloat16)
    shared_out = jnp.dot(shared_hidden, shared_down, preferred_element_type=jnp.float32)
    return (wide + shared_out + routed).astype(jnp.bfloat16)


def solution(mesh):
    in_specs = (
        P(("sp", "tp"), None),
        P("sp", "tp"),
        P("sp", "tp"),
        P("sp", "tp"),
        P("sp", "tp"),
        P("tp", None),
        P(),
        P(("sp", "tp"), None),
        P(("sp", "tp"), None),
        P("sp", None, None),
        P("sp", None, None),
        P("sp", None, None),
        P(),
        P(),
        P(),
    )
    out_specs = P(("sp", "tp"), None)
    return jax.shard_map(local, mesh=mesh, in_specs=in_specs, out_specs=out_specs, check_vma=False)
```

profile of v0, /device:TPU:0, one launch (start us, length us, event | category | flops | bytes accessed | tf_op | source)
XLA Modules:
  0.0 271.7 jit_solution(16404299911886271078)
XLA Ops:
  6.5 1.8 copy.30
  11.8 33.0 %all_gather.10 = f32[2048,4]{0,1:T(4,128)S(1)} all-gather(f32[256,4]{0,1:T(4,128)} %param.23), channel_id=1, replica_groups=mesh['sp'=8,'tp'=4] {'sp'}, dimensions={0}, use_global_device_ids=true | all-gather | bytes 36864 | tf_op jit(solution)/shard_map/all_gather | solution.py:89
  44.8 6.7 %all-gather.3.cloned.1.call-done = bf16[2048,256]{0,1:T(8,128)(2,1)} async-done(((bf16[256,256]{0,1:T(8,128)(2,1)}), bf16[2048,256]{0,1:T(8,128)(2,1)}) %all-gather.3.cloned.1.call-update) | async-done | bytes 1048592 | tf_op jit(solution)/shard_map/all_gather | solution.py:119
  51.5 2.3 copy.33
  53.8 39.2 %all-gather.5.cloned.1.call-done = bf16[2048,256]{1,0:T(8,128)(2,1)} async-done(((bf16[256,256]{1,0:T(8,128)(2,1)}), bf16[2048,256]{1,0:T(8,128)(2,1)}) %all-gather.5.cloned.1.call-update) | async-done | bytes 1048592 | tf_op jit(solution)/shard_map/all_gather | solution.py:120
  93.0 2.3 copy.32
  95.3 7.0 %while.18 = (s32[]{:T(128)}, f32[2,2,256]{2,1,0:T(2,128)S(1)}, f32[2,2,256]{2,1,0:T(2,128)S(1)}, f32[256,2,2,128]{0,3,2,1:T(8,128)S(1)}, s32[]{:T(128)}, /*index...) while((s32[]{:T(128)}, f32[2,2,256]{2,1,0:T(2,128)S(1)}, ...), condition=%wide.region_5.6_spmd.clone, body=%wide.region_0.5_spmd.clone.sunk | while | flops 555225344 | bytes 20357496 | solution.py:56
  96.0 5.7 %conditional.3 = ((f32[2,2,256]{2,1,0:T(2,128)S(1)}, f32[2,2,256]{2,1,0:T(2,128)S(1)}, f32[256,2,2,128]{0,3,2,1:T(8,128)S(1)})) conditional(s32[]{:T(128)} %convert_element_type.127, (f32[2,2,256]{2,1,0:T(2,128)S(1)}, f32[2,2,256]{2,1,0:T(2,128)S(1)}, f32[256,2,2,128]{0,3,2,1:T(8,128)S(1)}) %tuple.46, (s32[]{:T(128)}, s32[]{:T(128)}, ...), branch_computations={%region_1.0_spmd, %region_2.4_spmd} | conditional | flops 555225344 | bytes 20356210 | solution.py:54
  96.3 2.3 fusion.5
  98.6 1.6 fusion.12
  100.2 1.4 fusion.4
  102.4 1.7 convolution_convert_fusion.1
  105.7 1.4 scatter_custom_fusion
  107.1 26.4 %reduce-scatter.2.cloned.1.call-done = bf16[64,2048]{1,0:T(8,128)(2,1)} async-done(((bf16[256,2048]{1,0:T(8,128)(2,1)}), bf16[64,2048]{1,0:T(8,128)(2,1)}) %reduce-scatter.2.cloned.1.call-update) | async-done | bytes 262160 | tf_op jit(solution)/shard_map/reduce_scatter | solution.py:126
  134.9 3.3 %gather_fusion = bf16[512,2048]{1,0:T(8,128)(2,1)} fusion(bf16[65,2048]{1,0:T(8,128)(2,1)S(1)} %concatenate.3, s32[1024]{0:T(1024)S(1)} %pad_clamp_fusion.1), kind=kCustom, calls=%fused_computation | custom fusion | bytes 4196352 | tf_op jit(solution)/shard_map/gather | solution.py:155
  138.2 53.7 %all_to_all.10 = bf16[8,1,64,2048]{3,2,1,0:T(8,128)(2,1)S(1)} all-to-all(bf16[8,1,64,2048]{3,2,1,0:T(8,128)(2,1)} %bitcast.136), channel_id=1, replica_groups=mesh['sp'=8,'tp'=4] {'sp'}, dimensions={0} | all-to-all | bytes 4194304 | tf_op jit(solution)/shard_map/all_to_all | solution.py:156
  194.5 6.2 %fusion.25 = bf16[8,1,64,2048]{3,2,1,0:T(8,128)(2,1)} fusion(bf16[1,384,2048]{2,1,0:T(8,128)(2,1)} %param.30, bf16[1,2048,384]{2,1,0:T(8,128)(2,1)} %param.29, bf16[8,1,64,2048]{3,2,1,0:T(8,128)(2,1)} %copy-done.1, f32[8,1,64,384]{3,2,0,1:T(8,128)S(1)} %fusion.35), kind=kOutput, calls=%fused_computation.31 | convolution fusion | flops 1612840960 | bytes 8126464 | tf_op jit(solution)/shard_map/necf,efd->necd/dot_general | solution.py:162
  200.7 4.7 %all-to-all-start.1 = ((bf16[8,1,64,2048]{3,2,1,0:T(8,128)(2,1)}), bf16[8,1,64,2048]{3,2,1,0:T(8,128)(2,1)}, u32[]{:S(2)}, u32[]{:S(2)}) async-start(bf16[8,1,64,2048]{3,2,1,0:T(8,128)(2,1)} %fusion.25), calls=%async_computation.2 | async-start | bytes 4194304 | tf_op jit(solution)/shard_map/all_to_all | solution.py:165
  205.6 1.8 fusion.85
  207.4 45.2 %all-to-all-done.1 = bf16[8,1,64,2048]{3,2,1,0:T(8,128)(2,1)} async-done(((bf16[8,1,64,2048]{3,2,1,0:T(8,128)(2,1)}), bf16[8,1,64,2048]{3,2,1,0:T(8,128)(2,1)}, u32[]{:S(2)}, u32[]{:S(2)}) %all-to-all-start.1) | async-done | bytes 2097184 | tf_op jit(solution)/shard_map/all_to_all | solution.py:165
  252.6 4.2 %gather_fusion.1 = bf16[256,2048]{1,0:T(8,128)(2,1)S(1)} fusion(bf16[512,2048]{1,0:T(8,128)(2,1)} %bitcast.41, s32[1024]{0:T(1024)S(1)} %pad_clamp_fusion), kind=kCustom, calls=%fused_computation.1 | custom fusion | bytes 2098176 | tf_op jit(solution)/shard_map/gather | solution.py:167
  256.8 1.7 reshape.128
  258.5 3.2 %multiply_reduce_fusion = f32[64,2048]{1,0:T(8,128)S(1)} fusion(f32[64,4,2048]{2,1,0:T(4,128)} %reshape.128, f32[64,4]{1,0:T(8,128)S(1)} %copy.35), kind=kLoop, calls=%fused_computation.40 | loop fusion | flops 917504 | bytes 2622464 | tf_op jit(solution)/shard_map/reduce_sum | solution.py:169
  261.7 3.4 %fusion.27 = bf16[64,2048]{1,0:T(8,128)(2,1)} fusion(f32[64,2048]{1,0:T(8,128)S(1)} %multiply_reduce_fusion, bf16[384,2048]{1,0:T(8,128)(2,1)} %param.33, bf16[2048,384]{1,0:T(8,128)(2,1)} %param.32, bf16[64,2048]{1,0:T(8,128)(2,1)S(1)} %add_convert_fusion, f32[64,384]{1,0:T(8,128)S(1)} %fusion.85, f32[2048]{0:T(1024)S(1)} %copy-done.4, ...), kind=kOutput, calls=%fused_computation.35 | convolution fusion | flops 202522624 | bytes 4301056 | tf_op jit(solution)/shard_map/dot_general | solution.py:174
  (68 shorter events, 9.3 us)
Async XLA Ops:
  6.5 95.8 %copy-start = (bf16[512,2048]{1,0:T(8,128)(2,1)S(1)}, bf16[512,2048]{1,0:T(8,128)(2,1)}, u32[]{:S(2)}) copy-start(bf16[512,2048]{1,0:T(8,128)(2,1)} %param.24) | copy-start | bytes 6291460
  6.5 45.0 %all-gather.3.cloned.1.call-start = ((), (), s32[]{:S(2)}) async-start(), calls=%async_computation.3 | async-start | bytes 1179648 | tf_op jit(solution)/shard_map/all_gather | solution.py:119
  8.4 84.6 %all-gather.5.cloned.1.call-start = ((), (), s32[]{:S(2)}) async-start(), calls=%async_computation.4 | async-start | bytes 1179648 | tf_op jit(solution)/shard_map/all_gather | solution.py:120
  9.1 124.4 %reduce-scatter.2.cloned.1.call-start = ((), (), s32[]{:S(2)}) async-start(), calls=%async_computation.5 | async-start | bytes 1310720 | tf_op jit(solution)/shard_map/reduce_scatter | solution.py:126
  96.2 2.4 copy-start.2
  102.4 1.8 copy-start.5
  102.4 31.1 %copy-start.3 = (bf16[64,2048]{1,0:T(8,128)(2,1)S(1)}, bf16[64,2048]{1,0:T(8,128)(2,1)}, u32[]{:S(2)}) copy-start(bf16[64,2048]{1,0:T(8,128)(2,1)} %param.19) | copy-start | bytes 786436
  102.4 32.3 %copy-start.4 = (f32[2048]{0:T(1024)S(1)}, f32[2048]{0:T(1024)}, u32[]{:S(2)}) copy-start(f32[2048]{0:T(1024)} %param.25) | copy-start | bytes 24580
  138.2 55.0 %copy-start.7 = (bf16[1,2048,384]{2,1,0:T(8,128)(2,1)S(1)}, bf16[1,2048,384]{2,1,0:T(8,128)(2,1)}, u32[]{:S(2)}) copy-start(bf16[1,2048,384]{2,1,0:T(8,128)(2,1)} %param.28) | copy-start | bytes 4718596
  191.9 1.3 copy-start.1
  200.7 4.7 %copy-start.6 = (f32[64,4]{0,1:T(4,128)S(1)}, f32[64,4]{0,1:T(4,128)}, u32[]{:S(2)}) copy-start(f32[64,4]{0,1:T(4,128)} %param.27) | copy-start | bytes 3076
  200.7 51.8 %all-to-all-start.1 = ((bf16[8,1,64,2048]{3,2,1,0:T(8,128)(2,1)}), bf16[8,1,64,2048]{3,2,1,0:T(8,128)(2,1)}, u32[]{:S(2)}, u32[]{:S(2)}) async-start(bf16[8,1,64,2048]{3,2,1,0:T(8,128)(2,1)} %fusion.25), calls=%async_computation.2 | async-start | bytes 4194304 | tf_op jit(solution)/shard_map/all_to_all | solution.py:165
Sparse Core Ops, SparseCore 0:
  9.4 42.1 all-gather.2
  53.7 39.2 all-gather.4
  104.3 29.1 reduce-scatter.1
where the time goes:
time: 272 us
  waiting for transfers between devices  118 us (43%)
  blocking collectives  86.7 us (32%)
  local copies, waits for them, and re-layouts  21.9 us (8%)
  matrix products  18.4 us (7%)
  between operations  13.3 us (5%)
  other arithmetic  6.9 us (3%)
  starting transfers between devices  4.77 us (2%)
    all_to_all x1, blocking collectives, local(): lax.all_to_all(outgoing, 'sp', split_axis=0, concat_axis=0, tiled=True)  53.7 us
    all_to_all x1, waiting for transfers between devices, local(): lax.all_to_all(processed, 'sp', split_axis=0, concat_axis=0, tiled=True)  45.2 us
    all_gather x1, waiting for transfers between devices, local(): lax.all_gather(value_rows, 'sp', axis=0, tiled=True)  39.2 us
    all_gather x1, blocking collectives, local(): all_sums = lax.all_gather(forget_sums, 'sp', axis=0, tiled=True)  33 us
    reduce_scatter x1, waiting for transfers between devices, local(): lax.psum_scatter(jnp.dot(attended, out_weight, preferred_element_type=jnp...  26.4 us
    unnamed x19, local copies, waits for them, and re-layouts  6.76 us
    all_gather x1, waiting for transfers between devices, local(): lax.all_gather(key_rows, 'sp', axis=0, tiled=True)  6.72 us
    dot_general x1, matrix products, local(): jnp.einsum('necf,efd->necd', hidden, expert_down, preferred_element_type=...  6.24 us
  transfers between devices with their start and end apart: 4, of which 4 were waited for; matrix products, arithmetic and copies ran while one was open for 4% of the time, Pallas kernels for 0%

commit v1 on v0

--- a/solution.py
+++ b/solution.py
@@ -3,6 +3,7 @@
 import jax.numpy as jnp
 from jax import lax
 from jax.sharding import PartitionSpec as P
+from jax.lax import axis_index, axis_size, ppermute
 
 HEADS = 16
 KV_HEADS = 8
@@ -86,7 +87,16 @@
     group_size = HEADS // KV_HEADS
     score_scale = HEAD_DIM ** (-0.5)
     own_first = sp_index * local_rows
-    all_sums = lax.all_gather(forget_sums, "sp", axis=0, tiled=True)
+    axis_n = axis_size("sp")
+    aux = sorted(((j, (j + 1) % axis_n) for j in range(axis_n)))
+    x_next = forget_sums
+    found = [x_next]
+    for tick in tuple(range(1, axis_n)):
+        x_next = ppermute(x_next, "sp", aux)
+        found.insert(0, x_next)
+    block_now = jnp.concatenate(found, axis=0)
+    built = axis_index("sp")
+    all_sums = jnp.roll(block_now, (built + 1) * forget_sums.shape[0], axis=0)
     positions = own_first + jnp.arange(local_rows, dtype=jnp.int32)
     groups = [
         (

time: 272 us -> 273 us (level)
  blocking collectives: 86.7 us -> 53.7 us
  waiting for transfers between devices: 118 us -> 147 us
  starting transfers between devices: 4.77 us -> 7.85 us
    ppermute x0 -> x7, waiting for transfers between devices: none -> 40.2 us  [local(): x_next = ppermute(x_next, 'sp', aux)]
    all_gather x1 -> x0, blocking collectives: 33 us -> none  [local(): all_sums = lax.all_gather(forget_sums, 'sp', axis=0, tiled=True)]
    all_gather x1, waiting for transfers between devices: 6.72 us -> 0.02 us  [local(): lax.all_gather(key_rows, 'sp', axis=0, tiled=True)]
    all_gather x1, waiting for transfers between devices: 39.2 us -> 34.8 us  [local(): lax.all_gather(value_rows, 'sp', axis=0, tiled=True)]
    ppermute x0 -> x7, starting transfers between devices: none -> 3.06 us  [local(): x_next = ppermute(x_next, 'sp', aux)]
    unnamed x19 -> x34, local copies, waits for them, and re-layouts: 6.76 us -> 7.58 us
  transfers between devices with their start and end apart: 4 -> 11, of which waited for: 4 -> 10; matrix products, arithmetic and copies ran while one was open for 4% -> 4% of each run, Pallas kernels for 0% -> 0%
where the time goes in v1:
time: 273 us; the launch traced here: 272 us
  waiting for transfers between devices  147 us (54%)
  blocking collectives  53.7 us (20%)
  local copies, waits for them, and re-layouts  23.5 us (9%)
  matrix products  18.4 us (7%)
  between operations  13.4 us (5%)
  starting transfers between devices  7.85 us (3%)
  other arithmetic  6.9 us (3%)
    all_to_all x1, blocking collectives, local(): lax.all_to_all(outgoing, 'sp', split_axis=0, concat_axis=0, tiled=True)  53.7 us
    all_to_all x1, waiting for transfers between devices, local(): lax.all_to_all(processed, 'sp', split_axis=0, concat_axis=0, tiled=True)  45.2 us
    ppermute x7, waiting for transfers between devices, local(): x_next = ppermute(x_next, 'sp', aux)  40.2 us
    all_gather x1, waiting for transfers between devices, local(): lax.all_gather(value_rows, 'sp', axis=0, tiled=True)  34.8 us
    reduce_scatter x1, waiting for transfers between devices, local(): lax.psum_scatter(jnp.dot(attended, out_weight, preferred_element_type=jnp...  26.4 us
    unnamed x34, local copies, waits for them, and re-layouts  7.58 us
    dot_general x1, matrix products, local(): jnp.einsum('necf,efd->necd', hidden, expert_down, preferred_element_type=...  6.24 us
  transfers between devices with their start and end apart: 11, of which 10 were waited for; matrix products, arithmetic and copies ran while one was open for 4% of the time, Pallas kernels for 0%

profile of v1, /device:TPU:0, one launch (start us, length us, event | category | flops | bytes accessed | tf_op | source)
XLA Modules:
  0.0 271.9 jit_solution(6082530103357456302)
XLA Ops:
  8.4 3.0 %collective-permute-start = (f32[256,4]{0,1:T(4,128)}, f32[256,4]{0,1:T(4,128)S(1)}, u32[]{:S(2)}, u32[]{:S(2)}) collective-permute-start(f32[256,4]{0,1:T(4,128)} %param.23), channel_id=1, source_target_pairs={{0,4},{4,8},{8,12},{12,16},{16,20},{20,24},{24,28},{28,0},{1,5},{5... | collective-permute-start | bytes 12296 | tf_op jit(solution)/shard_map/ppermute | solution.py:95
  11.5 4.8 %collective-permute-done = f32[256,4]{0,1:T(4,128)S(1)} collective-permute-done((f32[256,4]{0,1:T(4,128)}, f32[256,4]{0,1:T(4,128)S(1)}, u32[]{:S(2)}, u32[]{:S(2)}) %collective-permute-start) | collective-permute-done | bytes 4128 | tf_op jit(solution)/shard_map/ppermute | solution.py:95
  16.3 6.3 %collective-permute-done.1 = f32[256,4]{0,1:T(4,128)S(1)} collective-permute-done((f32[256,4]{0,1:T(4,128)S(1)}, f32[256,4]{0,1:T(4,128)S(1)}, u32[]{:S(2)}, u32[]{:S(2)}) %collective-permute-start.1) | collective-permute-done | bytes 4128 | tf_op jit(solution)/shard_map/ppermute | solution.py:95
  22.6 6.3 %collective-permute-done.2 = f32[256,4]{0,1:T(4,128)S(1)} collective-permute-done((f32[256,4]{0,1:T(4,128)S(1)}, f32[256,4]{0,1:T(4,128)S(1)}, u32[]{:S(2)}, u32[]{:S(2)}) %collective-permute-start.2) | collective-permute-done | bytes 4128 | tf_op jit(solution)/shard_map/ppermute | solution.py:95
  28.9 6.3 %collective-permute-done.3 = f32[256,4]{0,1:T(4,128)S(1)} collective-permute-done((f32[256,4]{0,1:T(4,128)S(1)}, f32[256,4]{0,1:T(4,128)S(1)}, u32[]{:S(2)}, u32[]{:S(2)}) %collective-permute-start.3) | collective-permute-done | bytes 4128 | tf_op jit(solution)/shard_map/ppermute | solution.py:95
  35.2 6.4 %collective-permute-done.4 = f32[256,4]{0,1:T(4,128)S(1)} collective-permute-done((f32[256,4]{0,1:T(4,128)S(1)}, f32[256,4]{0,1:T(4,128)S(1)}, u32[]{:S(2)}, u32[]{:S(2)}) %collective-permute-start.4) | collective-permute-done | bytes 4128 | tf_op jit(solution)/shard_map/ppermute | solution.py:95
  41.7 6.4 %collective-permute-done.5 = f32[256,4]{0,1:T(4,128)S(1)} collective-permute-done((f32[256,4]{0,1:T(4,128)S(1)}, f32[256,4]{0,1:T(4,128)S(1)}, u32[]{:S(2)}, u32[]{:S(2)}) %collective-permute-start.5) | collective-permute-done | bytes 4128 | tf_op jit(solution)/shard_map/ppermute | solution.py:95
  50.7 3.7 %collective-permute-done.6 = f32[256,4]{0,1:T(4,128)S(1)} collective-permute-done((f32[256,4]{0,1:T(4,128)S(1)}, f32[256,4]{0,1:T(4,128)S(1)}, u32[]{:S(2)}, u32[]{:S(2)}) %collective-permute-start.6) | collective-permute-done | bytes 4128 | tf_op jit(solution)/shard_map/ppermute | solution.py:95
  56.0 2.3 copy.33
  58.2 34.8 %all-gather.5.cloned.1.call-done = bf16[2048,256]{1,0:T(8,128)(2,1)} async-done(((bf16[256,256]{1,0:T(8,128)(2,1)}), bf16[2048,256]{1,0:T(8,128)(2,1)}) %all-gather.5.cloned.1.call-update) | async-done | bytes 1048592 | tf_op jit(solution)/shard_map/all_gather | solution.py:130
  93.1 2.3 copy.32
  95.4 7.1 %while.18 = (s32[]{:T(128)}, f32[2,2,256]{2,1,0:T(2,128)S(1)}, f32[2,2,256]{2,1,0:T(2,128)S(1)}, f32[256,2,2,128]{0,3,2,1:T(8,128)S(1)}, s32[]{:T(128)}, /*index...) while((s32[]{:T(128)}, f32[2,2,256]{2,1,0:T(2,128)S(1)}, ...), condition=%wide.region_5.6_spmd.clone, body=%wide.region_0.5_spmd.clone.sunk | while | flops 555225344 | bytes 20357496 | solution.py:57
  96.1 5.7 %conditional.3 = ((f32[2,2,256]{2,1,0:T(2,128)S(1)}, f32[2,2,256]{2,1,0:T(2,128)S(1)}, f32[256,2,2,128]{0,3,2,1:T(8,128)S(1)})) conditional(s32[]{:T(128)} %convert_element_type.127, (f32[2,2,256]{2,1,0:T(2,128)S(1)}, f32[2,2,256]{2,1,0:T(2,128)S(1)}, f32[256,2,2,128]{0,3,2,1:T(8,128)S(1)}) %tuple.46, (s32[]{:T(128)}, s32[]{:T(128)}, ...), branch_computations={%region_1.1_spmd, %region_2.4_spmd} | conditional | flops 555225344 | bytes 20356210 | solution.py:55
  96.4 2.3 fusion.5
  107.4 26.4 %reduce-scatter.2.cloned.1.call-done = bf16[64,2048]{1,0:T(8,128)(2,1)} async-done(((bf16[256,2048]{1,0:T(8,128)(2,1)}), bf16[64,2048]{1,0:T(8,128)(2,1)}) %reduce-scatter.2.cloned.1.call-update) | async-done | bytes 262160 | tf_op jit(solution)/shard_map/reduce_scatter | solution.py:136
  135.1 3.3 %gather_fusion = bf16[512,2048]{1,0:T(8,128)(2,1)} fusion(bf16[65,2048]{1,0:T(8,128)(2,1)S(1)} %concatenate.10, s32[1024]{0:T(1024)S(1)} %pad_clamp_fusion.1), kind=kCustom, calls=%fused_computation | custom fusion | bytes 4196352 | tf_op jit(solution)/shard_map/gather | solution.py:165
  138.4 53.7 %all_to_all.10 = bf16[8,1,64,2048]{3,2,1,0:T(8,128)(2,1)S(1)} all-to-all(bf16[8,1,64,2048]{3,2,1,0:T(8,128)(2,1)} %bitcast.136), channel_id=1, replica_groups=mesh['sp'=8,'tp'=4] {'sp'}, dimensions={0} | all-to-all | bytes 4194304 | tf_op jit(solution)/shard_map/all_to_all | solution.py:166
  194.7 6.2 %fusion.25 = bf16[8,1,64,2048]{3,2,1,0:T(8,128)(2,1)} fusion(bf16[1,384,2048]{2,1,0:T(8,128)(2,1)} %param.30, bf16[1,2048,384]{2,1,0:T(8,128)(2,1)} %param.29, bf16[8,1,64,2048]{3,2,1,0:T(8,128)(2,1)} %copy-done.1, f32[8,1,64,384]{3,2,0,1:T(8,128)S(1)} %fusion.35), kind=kOutput, calls=%fused_computation.31 | convolution fusion | flops 1612840960 | bytes 8126464 | tf_op jit(solution)/shard_map/necf,efd->necd/dot_general | solution.py:172
  200.9 4.7 %all-to-all-start.1 = ((bf16[8,1,64,2048]{3,2,1,0:T(8,128)(2,1)}), bf16[8,1,64,2048]{3,2,1,0:T(8,128)(2,1)}, u32[]{:S(2)}, u32[]{:S(2)}) async-start(bf16[8,1,64,2048]{3,2,1,0:T(8,128)(2,1)} %fusion.25), calls=%async_computation.2 | async-start | bytes 4194304 | tf_op jit(solution)/shard_map/all_to_all | solution.py:175
  205.8 1.8 fusion.85
  207.6 45.2 %all-to-all-done.1 = bf16[8,1,64,2048]{3,2,1,0:T(8,128)(2,1)} async-done(((bf16[8,1,64,2048]{3,2,1,0:T(8,128)(2,1)}), bf16[8,1,64,2048]{3,2,1,0:T(8,128)(2,1)}, u32[]{:S(2)}, u32[]{:S(2)}) %all-to-all-start.1) | async-done | bytes 2097184 | tf_op jit(solution)/shard_map/all_to_all | solution.py:175
  252.8 4.2 %gather_fusion.1 = bf16[256,2048]{1,0:T(8,128)(2,1)S(1)} fusion(bf16[512,2048]{1,0:T(8,128)(2,1)} %bitcast.41, s32[1024]{0:T(1024)S(1)} %pad_clamp_fusion), kind=kCustom, calls=%fused_computation.1 | custom fusion | bytes 2098176 | tf_op jit(solution)/shard_map/gather | solution.py:177
  258.8 3.2 %multiply_reduce_fusion = f32[64,2048]{1,0:T(8,128)S(1)} fusion(f32[64,4,2048]{2,1,0:T(4,128)} %reshape.128, f32[64,4]{1,0:T(8,128)S(1)} %copy.35), kind=kLoop, calls=%fused_computation.40 | loop fusion | flops 917504 | bytes 2622464 | tf_op jit(solution)/shard_map/reduce_sum | solution.py:179
  261.9 3.4 %fusion.27 = bf16[64,2048]{1,0:T(8,128)(2,1)} fusion(f32[64,2048]{1,0:T(8,128)S(1)} %multiply_reduce_fusion, bf16[384,2048]{1,0:T(8,128)(2,1)} %param.33, bf16[2048,384]{1,0:T(8,128)(2,1)} %param.32, bf16[64,2048]{1,0:T(8,128)(2,1)S(1)} %add_convert_fusion, f32[64,384]{1,0:T(8,128)S(1)} %fusion.85, f32[2048]{0:T(1024)S(1)} %copy-done.4, ...), kind=kOutput, calls=%fused_computation.35 | convolution fusion | flops 202522624 | bytes 4301056 | tf_op jit(solution)/shard_map/dot_general | solution.py:184
  (98 shorter events, 19.8 us)
Async XLA Ops:
  6.5 96.1 %copy-start = (bf16[512,2048]{1,0:T(8,128)(2,1)S(1)}, bf16[512,2048]{1,0:T(8,128)(2,1)}, u32[]{:S(2)}) copy-start(bf16[512,2048]{1,0:T(8,128)(2,1)} %param.24) | copy-start | bytes 6291460
  6.5 49.4 %all-gather.3.cloned.1.call-start = ((), (), s32[]{:S(2)}) async-start(), calls=%async_computation.3 | async-start | bytes 1179648 | tf_op jit(solution)/shard_map/all_gather | solution.py:129
  8.4 84.7 %all-gather.5.cloned.1.call-start = ((), (), s32[]{:S(2)}) async-start(), calls=%async_computation.4 | async-start | bytes 1179648 | tf_op jit(solution)/shard_map/all_gather | solution.py:130
  8.4 7.9 %collective-permute-start = (f32[256,4]{0,1:T(4,128)}, f32[256,4]{0,1:T(4,128)S(1)}, u32[]{:S(2)}, u32[]{:S(2)}) collective-permute-start(f32[256,4]{0,1:T(4,128)} %param.23), channel_id=1, source_target_pairs={{0,4},{4,8},{8,12},{12,16},{16,20},{20,24},{24,28},{28,0},{1,5},{5... | collective-permute-start | bytes 12296 | tf_op jit(solution)/shard_map/ppermute | solution.py:95
  16.3 6.3 %collective-permute-start.1 = (f32[256,4]{0,1:T(4,128)S(1)}, f32[256,4]{0,1:T(4,128)S(1)}, u32[]{:S(2)}, u32[]{:S(2)}) collective-permute-start(f32[256,4]{0,1:T(4,128)S(1)} %collective-permute-done), channel_id=1, source_target_pairs={{0,4},{4,8},{8,12},{12,16},{16,20},{20,24},{24,28},{28,0},{1,5},{5... | collective-permute-start | bytes 12296 | tf_op jit(solution)/shard_map/ppermute | solution.py:95
  22.6 6.3 %collective-permute-start.2 = (f32[256,4]{0,1:T(4,128)S(1)}, f32[256,4]{0,1:T(4,128)S(1)}, u32[]{:S(2)}, u32[]{:S(2)}) collective-permute-start(f32[256,4]{0,1:T(4,128)S(1)} %collective-permute-done.1), channel_id=1, source_target_pairs={{0,4},{4,8},{8,12},{12,16},{16,20},{20,24},{24,28},{28,0},{1,5},{5... | collective-permute-start | bytes 12296 | tf_op jit(solution)/shard_map/ppermute | solution.py:95
  28.9 6.3 %collective-permute-start.3 = (f32[256,4]{0,1:T(4,128)S(1)}, f32[256,4]{0,1:T(4,128)S(1)}, u32[]{:S(2)}, u32[]{:S(2)}) collective-permute-start(f32[256,4]{0,1:T(4,128)S(1)} %collective-permute-done.2), channel_id=1, source_target_pairs={{0,4},{4,8},{8,12},{12,16},{16,20},{20,24},{24,28},{28,0},{1,5},{5... | collective-permute-start | bytes 12296 | tf_op jit(solution)/shard_map/ppermute | solution.py:95
  35.2 6.4 %collective-permute-start.4 = (f32[256,4]{0,1:T(4,128)S(1)}, f32[256,4]{0,1:T(4,128)S(1)}, u32[]{:S(2)}, u32[]{:S(2)}) collective-permute-start(f32[256,4]{0,1:T(4,128)S(1)} %collective-permute-done.3), channel_id=1, source_target_pairs={{0,4},{4,8},{8,12},{12,16},{16,20},{20,24},{24,28},{28,0},{1,5},{5... | collective-permute-start | bytes 12296 | tf_op jit(solution)/shard_map/ppermute | solution.py:95
  41.6 6.4 %collective-permute-start.5 = (f32[256,4]{0,1:T(4,128)S(1)}, f32[256,4]{0,1:T(4,128)S(1)}, u32[]{:S(2)}, u32[]{:S(2)}) collective-permute-start(f32[256,4]{0,1:T(4,128)S(1)} %collective-permute-done.4), channel_id=1, source_target_pairs={{0,4},{4,8},{8,12},{12,16},{16,20},{20,24},{24,28},{28,0},{1,5},{5... | collective-permute-start | bytes 12296 | tf_op jit(solution)/shard_map/ppermute | solution.py:95
  41.7 92.1 %reduce-scatter.2.cloned.1.call-start = ((), (), s32[]{:S(2)}) async-start(), calls=%async_computation.5 | async-start | bytes 1310720 | tf_op jit(solution)/shard_map/reduce_scatter | solution.py:136
  48.1 6.3 %collective-permute-start.6 = (f32[256,4]{0,1:T(4,128)S(1)}, f32[256,4]{0,1:T(4,128)S(1)}, u32[]{:S(2)}, u32[]{:S(2)}) collective-permute-start(f32[256,4]{0,1:T(4,128)S(1)} %collective-permute-done.5), channel_id=1, source_target_pairs={{0,4},{4,8},{8,12},{12,16},{16,20},{20,24},{24,28},{28,0},{1,5},{5... | collective-permute-start | bytes 12296 | tf_op jit(solution)/shard_map/ppermute | solution.py:95
  96.4 2.4 copy-start.2
  102.6 1.8 copy-start.5
  102.6 31.1 %copy-start.3 = (bf16[64,2048]{1,0:T(8,128)(2,1)S(1)}, bf16[64,2048]{1,0:T(8,128)(2,1)}, u32[]{:S(2)}) copy-start(bf16[64,2048]{1,0:T(8,128)(2,1)} %param.19) | copy-start | bytes 786436
  102.7 32.3 %copy-start.4 = (f32[2048]{0:T(1024)S(1)}, f32[2048]{0:T(1024)}, u32[]{:S(2)}) copy-start(f32[2048]{0:T(1024)} %param.25) | copy-start | bytes 24580
  138.4 55.0 %copy-start.7 = (bf16[1,2048,384]{2,1,0:T(8,128)(2,1)S(1)}, bf16[1,2048,384]{2,1,0:T(8,128)(2,1)}, u32[]{:S(2)}) copy-start(bf16[1,2048,384]{2,1,0:T(8,128)(2,1)} %param.28) | copy-start | bytes 4718596
  192.1 1.3 copy-start.1
  200.9 4.7 %copy-start.6 = (f32[64,4]{0,1:T(4,128)S(1)}, f32[64,4]{0,1:T(4,128)}, u32[]{:S(2)}) copy-start(f32[64,4]{0,1:T(4,128)} %param.27) | copy-start | bytes 3076
  200.9 51.9 %all-to-all-start.1 = ((bf16[8,1,64,2048]{3,2,1,0:T(8,128)(2,1)}), bf16[8,1,64,2048]{3,2,1,0:T(8,128)(2,1)}, u32[]{:S(2)}, u32[]{:S(2)}) async-start(bf16[8,1,64,2048]{3,2,1,0:T(8,128)(2,1)} %fusion.25), calls=%async_computation.2 | async-start | bytes 4194304 | tf_op jit(solution)/shard_map/all_to_all | solution.py:175
Sparse Core Ops, SparseCore 0:
  9.4 42.0 all-gather.2
  53.6 39.4 all-gather.4
  104.5 29.1 reduce-scatter.1
